TPU v7x, 32 devices: a whole 2x2x4 slice. The times are simulated.
32 devices in a mesh: gr: 2 (over y), fs: 8 (over z, core), tp: 2 (over x).
Axes of the slice: x: 2, y: 2, z: 4, core: 2. Of those that a mesh axis runs over, the one named last changes fastest.
Arguments:
- prompt: bfloat16 [2048, 2048], P(('gr', 'fs')), may hold values from -6 to 6
- expert_ids: int32 [2048, 2], P(('gr', 'fs')), may hold values from 0 to 7, all different within a row; in each aligned block of 128 rows (0 to 127, 128 to 255, ...) at most 32 rows name the same one
- route_weights: float32 [2048, 2], P(('gr', 'fs')), may hold values from 0.2 to 1
- gate_master: float32 [8, 2048, 8192], P('gr', 'fs', 'tp'), may hold values from -0.125 to 0.125
- up_master: float32 [8, 2048, 8192], P('gr', 'fs', 'tp'), may hold values from -0.125 to 0.125
- down_master: float32 [8, 8192, 2048], P('gr', 'fs', 'tp'), may hold values from -0.0625 to 0.0625
- ffn_gain: float32 [2048], P('fs'), may hold values from 0.1 to 1.9
Outputs:
- gate_serving: bfloat16 [8, 2048, 8192], P('tp', None, 'fs')
- up_serving: bfloat16 [8, 2048, 8192], P('tp', None, 'fs')
- down_serving: bfloat16 [8, 8192, 2048], P('tp', 'fs')
- mixed: bfloat16 [2048, 2048], P(('gr', 'fs', 'tp'))
Inputs may be any that keep to these rules, and one draw needn't show every extreme that they name: `expert_ids`: the two experts of a token differ; the rows of one index of gr and fs name each expert exactly 32 times.
All inputs are finite; a program needn't handle non-finite values.
Results may differ from a plain program's by a relative error of at most 0.025.
Values may be sent and summed in bfloat16 or wider, within the bound.
A program may use at most 256 MiB of HBM per device.

v0:
```python
import jax
import jax.numpy as jnp
from jax import lax
from jax.sharding import PartitionSpec as P

EXPERTS = 8
SLOTS = 32


NORM_EPS = 1e-06


def regroup_rows(weights, group_count, shard_count):
    local_experts, row_total, width = weights.shape
    stacked = weights.reshape(
        local_experts, group_count, shard_count, row_total // (group_count * shard_count), width
    )
    return stacked.transpose(0, 2, 1, 3, 4).reshape(local_experts, row_total, width)


def body(prompt, expert_ids, route_weights, gate_master, up_master, down_master, ffn_gain):
    group_count = lax.axis_size("gr")
    shard_count = lax.axis_size("fs")
    folding = ffn_gain[None, :, None]
    gate_local = (gate_master * folding).astype(jnp.bfloat16)
    up_local = (up_master * folding).astype(jnp.bfloat16)
    down_local = down_master.astype(jnp.bfloat16)
    gate_rows, up_rows = (
        lax.all_to_all(gate_local, "gr", split_axis=1, concat_axis=0, tiled=True),
        lax.all_to_all(up_local, "gr", split_axis=1, concat_axis=0, tiled=True),
    )
    down_whole = lax.all_gather(down_local, "gr", axis=0, tiled=True)
    gate_cols, up_cols = (
        lax.all_to_all(
            lax.all_to_all(gate_rows, "tp", split_axis=0, concat_axis=2, tiled=True),
            "fs",
            split_axis=2,
            concat_axis=1,
            tiled=True,
        ),
        lax.all_to_all(
            lax.all_to_all(up_rows, "tp", split_axis=0, concat_axis=2, tiled=True),
            "fs",
            split_axis=2,
            concat_axis=1,
            tiled=True,
        ),
    )
    down_serving = lax.all_to_all(down_whole, "tp", split_axis=0, concat_axis=2, tiled=True)
    gate_joined, up_joined = (
        lax.all_gather(gate_cols, "gr", axis=1, tiled=True),
        lax.all_gather(up_cols, "gr", axis=1, tiled=True),
    )
    gate_serving = regroup_rows(gate_joined, group_count, shard_count)
    up_serving = regroup_rows(up_joined, group_count, shard_count)
    token_count = prompt.shape[0]
    local_experts = gate_serving.shape[0]
    xfloat = prompt.astype(jnp.float32)
    normed = (
        xfloat * lax.rsqrt(jnp.mean(xfloat * xfloat, axis=1, keepdims=True) + NORM_EPS)
    ).astype(jnp.bfloat16)
    first_expert = lax.axis_index("tp") * local_experts
    pair_expert = expert_ids.reshape(-1)
    expert_table = (pair_expert[:, None] == jnp.arange(EXPERTS, dtype=jnp.int32)[None, :]).astype(
        jnp.int32
    )
    ranking = jnp.sum((jnp.cumsum(expert_table, axis=0) - expert_table) * expert_table, axis=1)
    local_ids = pair_expert - first_expert
    pair_token = jnp.arange(pair_expert.shape[0], dtype=jnp.int32) // 2
    matched = (
        local_ids[None, None, :] == jnp.arange(local_experts, dtype=jnp.int32)[:, None, None]
    ) & (ranking[None, None, :] == jnp.arange(SLOTS, dtype=jnp.int32)[None, :, None])
    slot_token = jnp.sum(jnp.where(matched, pair_token[None, None, :], 0), axis=2)
    filled = jnp.any(matched, axis=2)
    routed = jnp.where(filled[:, :, None], normed[slot_token], jnp.zeros((), jnp.bfloat16))
    piece = lax.all_gather(routed, "fs", axis=1, tiled=True)
    gate_part = jnp.einsum("ecd,edf->ecf", piece, gate_serving, preferred_element_type=jnp.float32)
    up_part = jnp.einsum("ecd,edf->ecf", piece, up_serving, preferred_element_type=jnp.float32)
    hidden = (jax.nn.silu(gate_part) * up_part).astype(jnp.bfloat16)
    expert_out = lax.psum_scatter(
        jnp.einsum("ecf,efd->ced", hidden, down_serving, preferred_element_type=jnp.float32).astype(
            jnp.bfloat16
        ),
        "fs",
        scatter_dimension=0,
        tiled=True,
    ).astype(jnp.float32)
    is_local = (local_ids >= 0) & (local_ids < local_experts)
    safe_local = jnp.clip(local_ids, 0, local_experts - 1)
    safe_rank = jnp.minimum(ranking, SLOTS - 1)
    picked = expert_out[safe_rank, safe_local]
    weighted = jnp.where(
        is_local[:, None], picked * route_weights.reshape(-1)[:, None], 0.0
    ).astype(jnp.bfloat16)
    weighted = weighted.reshape(token_count, 2, weighted.shape[1])
    arrived = lax.all_to_all(weighted, "tp", split_axis=0, concat_axis=1, tiled=True)
    mixed = jnp.sum(arrived.astype(jnp.float32), axis=1).astype(jnp.bfloat16)
    return (gate_serving, up_serving, down_serving, mixed)


def solution(mesh):
    in_specs = (
        P(("gr", "fs"), None),
        P(("gr", "fs"), None),
        P(("gr", "fs"), None),
        P("gr", "fs", "tp"),
        P("gr", "fs", "tp"),
        P("gr", "fs", "tp"),
        P("fs"),
    )
    out_specs = (
        P("tp", None, "fs"),
        P("tp", None, "fs"),
        P("tp", "fs", None),
        P(("gr", "fs", "tp"), None),
    )
    return jax.shard_map(body, mesh=mesh, in_specs=in_specs, out_specs=out_specs, check_vma=False)
```

profile of v0, /device:TPU:0, one launch (start us, length us, event | category | flops | bytes accessed | tf_op | source)
XLA Modules:
  0.0 1267.4 jit_solution(1871464618973655169)
XLA Ops:
  7.2 15.1 %multiply_convert_fusion = (bf16[4,256,4096]{2,1,0:T(8,128)(2,1)}, bf16[4,256,4096]{2,1,0:T(8,128)(2,1)S(1)}) fusion(f32[4,256,4096]{2,1,0:T(8,128)} %param.11, f32[256]{0:T(256)} %param.13, f32[4,256,4096]{2,1,0:T(8,128)} %param.10), kind=kLoop, calls=%fused_computation.3 | loop fusion | flops 16777216 | bytes 50332672 | tf_op jit(solution)/shard_map/convert_element_type | solution.py:26
  22.3 12.6 copy.107
  34.9 98.2 %all_to_all.135 = bf16[4,256,4096]{2,0,1:T(4,128)(2,1)} all-to-all(bf16[4,256,4096]{2,0,1:T(4,128)(2,1)S(1)} %copy.107), channel_id=1, replica_groups=mesh['gr'=2,'fs'=8,'tp'=2] {'gr'}, dimensions={1} | all-to-all | bytes 16777216 | tf_op jit(solution)/shard_map/all_to_all | solution.py:29
  133.0 11.4 copy.108
  144.4 7.9 copy.109
  152.3 6.9 all-to-all-start.1
  159.2 12.2 copy.115
  171.4 79.9 %all-to-all-done.1 = bf16[8,128,4096]{2,1,0:T(8,128)(2,1)} async-done(((bf16[8,128,4096]{2,1,0:T(8,128)(2,1)}), bf16[8,128,4096]{2,1,0:T(8,128)(2,1)}, u32[]{:S(2)}, u32[]{:S(2)}) %all-to-all-start.1) | async-done | bytes 8388640 | tf_op jit(solution)/shard_map/all_to_all | solution.py:35
  251.2 7.0 all-to-all-start.3
  258.2 11.9 copy.110
  270.2 12.1 copy.111
  282.3 67.1 %all-to-all-done.3 = bf16[4,256,4096]{2,0,1:T(4,128)(2,1)} async-done(((bf16[4,256,4096]{2,0,1:T(4,128)(2,1)}), bf16[4,256,4096]{2,0,1:T(4,128)(2,1)}, u32[]{:S(2)}, u32[]{:S(2)}) %all-to-all-start.3) | async-done | bytes 8388640 | tf_op jit(solution)/shard_map/all_to_all | solution.py:30
  349.4 5.0 all-to-all-start.2
  354.4 0.2 all-gather.9.cloned.1.call-start
  354.6 9.1 convert_element_type.42
  363.7 13.5 %copy.116 = bf16[4,256,4096]{2,1,0:T(8,128)(2,1)} copy(bf16[4,256,4096]{2,0,1:T(4,128)(2,1)} %all-to-all-done.3) | data formatting | bytes 16777216 | tf_op jit(solution)/shard_map/all_to_all | solution.py:30
  377.1 9.3 copy.117
  386.5 151.8 %all-to-all-done.2 = bf16[4,128,8192]{1,0,2:T(4,128)(2,1)} async-done(((bf16[4,128,8192]{1,0,2:T(4,128)(2,1)}), bf16[4,128,8192]{1,0,2:T(4,128)(2,1)}, u32[]{:S(2)}, u32[]{:S(2)}) %all-to-all-start.2) | async-done | bytes 8388640 | tf_op jit(solution)/shard_map/all_to_all | solution.py:34
  538.2 7.0 all-to-all-start.4
  545.3 0.0 all-gather.5.cloned.1.call-start
  545.3 7.9 copy.112
  553.2 11.3 copy.113
  564.6 73.0 %all-to-all-done.4 = bf16[8,128,4096]{2,1,0:T(8,128)(2,1)} async-done(((bf16[8,128,4096]{2,1,0:T(8,128)(2,1)}), bf16[8,128,4096]{2,1,0:T(8,128)(2,1)}, u32[]{:S(2)}, u32[]{:S(2)}) %all-to-all-start.4) | async-done | bytes 8388640 | tf_op jit(solution)/shard_map/all_to_all | solution.py:42
  637.6 11.9 copy.118
  649.5 10.1 copy.119
  659.7 187.3 %all_to_all.136 = bf16[4,128,8192]{1,0,2:T(4,128)(2,1)} all-to-all(bf16[4,128,8192]{1,0,2:T(4,128)(2,1)S(1)} %copy.119), channel_id=1, replica_groups=mesh['gr'=2,'fs'=8,'tp'=2] {'fs'}, dimensions={2} | all-to-all | bytes 16777216 | tf_op jit(solution)/shard_map/all_to_all | solution.py:41
  847.0 7.9 copy.120
  854.8 11.3 copy.121
  866.2 0.7 copy-done.1
  866.8 0.1 copy.125
  866.9 0.1 eq.65
  867.1 0.1 reshape.196
  867.2 0.6 reduce-window.6
  867.8 0.2 slice_reduce_fusion
  868.1 0.1 fusion.7
  868.2 0.2 fusion.5
  868.4 0.1 reshape.200
  868.5 0.2 fusion.3
  868.7 13.3 %all-to-all-start.6 = ((bf16[8,1024,1024]{2,1,0:T(8,128)(2,1)}), bf16[8,1024,1024]{2,1,0:T(8,128)(2,1)}, u32[]{:S(2)}, u32[]{:S(2)}) async-start(bf16[8,1024,1024]{2,1,0:T(8,128)(2,1)} %all-gather.9.cloned.1.call-done), calls=%async_computation.6 | async-start | bytes 33554432 | tf_op jit(solution)/shard_map/all_to_all | solution.py:49
  882.0 0.0 all-gather.11.cloned.1.call-start
  882.0 0.2 fusion.4
  882.2 0.9 gather_fusion
  883.1 0.2 and_reduce_fusion
  883.3 1.0 broadcast_select_fusion
  884.3 0.0 reduce-scatter.2.cloned.1.call-start
  884.3 179.9 %all-to-all-done.6 = bf16[8,1024,1024]{2,1,0:T(8,128)(2,1)} async-done(((bf16[8,1024,1024]{2,1,0:T(8,128)(2,1)}), bf16[8,1024,1024]{2,1,0:T(8,128)(2,1)}, u32[]{:S(2)}, u32[]{:S(2)}) %all-to-all-start.6) | async-done | bytes 16777248 | tf_op jit(solution)/shard_map/all_to_all | solution.py:49
  1064.2 31.0 %copy.131 = bf16[2,4,1024,1024]{3,0,2,1:T(2,128)(2,1)} copy(bf16[2,4,1024,1024]{3,2,1,0:T(8,128)(2,1)} %bitcast.24) | data formatting | bytes 33554432 | tf_op jit(solution)/shard_map/all_to_all | solution.py:49
  1095.3 27.8 %all_to_all.125 = bf16[4,1024,2048]{2,1,0:T(8,128)(2,1)} reshape(bf16[4,1024,2,1024]{3,2,1,0:T(2,128)(2,1)} %bitcast.59) | data formatting | bytes 33554432 | tf_op jit(solution)/shard_map/all_to_all | solution.py:49
  1123.1 13.9 %copy.114 = bf16[4,8,2,128,1024]{4,3,2,1,0:T(8,128)(2,1)} copy(bf16[4,8,2,128,1024]{4,3,1,2,0:T(8,128)(2,1)} %bitcast.71) | data formatting | bytes 33554432 | tf_op jit(solution)/shard_map/transpose | solution.py:18
  1137.0 13.9 %copy.122 = bf16[4,8,2,128,1024]{4,3,2,1,0:T(8,128)(2,1)} copy(bf16[4,8,2,128,1024]{4,3,1,2,0:T(8,128)(2,1)} %bitcast.72) | data formatting | bytes 33554432 | tf_op jit(solution)/shard_map/transpose | solution.py:18
  1150.9 13.5 %fusion.15 = f32[4,256,1024]{2,1,0:T(8,128)} fusion(bf16[4,256,2048]{2,1,0:T(8,128)(2,1)} %all-gather.11.cloned.1.call-done, bf16[4,2048,1024]{2,1,0:T(8,128)(2,1)} %bitcast.73), kind=kOutput, calls=%fused_computation.46 | convolution fusion | flops 4294967296 | bytes 25165824 | tf_op jit(solution)/shard_map/ecd,edf->ecf/dot_general | solution.py:77
  1164.4 19.7 %convert_bitcast_fusion = bf16[256,4,2048]{2,0,1:T(8,128)(2,1)} fusion(bf16[4,1024,2048]{2,1,0:T(8,128)(2,1)} %all_to_all.125, f32[4,256,1024]{2,1,0:T(8,128)} %fusion.15, bf16[4,256,2048]{2,1,0:T(8,128)(2,1)} %all-gather.11.cloned.1.call-done, bf16[4,2048,1024]{2,1,0:T(8,128)(2,1)} %bitcast.75), kind=kOutput, calls=%fused_computation.5 | convolution fusion | flops 8598323200 | bytes 46137344 | tf_op jit(solution)/shard_map/ecf,efd->ced/dot_general | solution.py:81
  1184.2 0.1 copy.127
  1184.3 0.1 min.31
  1184.4 0.1 copy.124
  1184.6 0.1 copy.129
  1184.7 47.2 %reduce-scatter.2.cloned.1.call-done = bf16[32,4,2048]{2,0,1:T(8,128)(2,1)} async-done(((bf16[256,4,2048]{2,0,1:T(8,128)(2,1)}), bf16[32,4,2048]{2,0,1:T(8,128)(2,1)}) %reduce-scatter.2.cloned.1.call-update) | async-done | bytes 524304 | tf_op jit(solution)/shard_map/reduce_scatter | solution.py:80
  1231.9 1.4 copy.128
  1233.4 4.2 gather_fusion.1
  1237.6 2.3 gather.10
  1239.9 2.4 select_convert_fusion
  1242.2 14.5 %all_to_all.137 = bf16[128,2,2048]{2,1,0:T(2,128)(2,1)S(1)} all-to-all(bf16[128,2,2048]{2,1,0:T(2,128)(2,1)S(1)} %select_convert_fusion), channel_id=1, replica_groups=mesh['gr'=2,'fs'=8,'tp'=2] {'tp'}, dimensions={0} | all-to-all | bytes 2097152 | tf_op jit(solution)/shard_map/all_to_all | solution.py:96
  1256.7 2.8 reduce_sum.52
  1259.5 0.8 reduce_sum.54
  (29 shorter events, 0.3 us)
Async XLA Ops:
  152.3 99.0 %all-to-all-start.1 = ((bf16[8,128,4096]{2,1,0:T(8,128)(2,1)}), bf16[8,128,4096]{2,1,0:T(8,128)(2,1)}, u32[]{:S(2)}, u32[]{:S(2)}) async-start(bf16[8,128,4096]{2,1,0:T(8,128)(2,1)} %bitcast.63), calls=%async_computation.1 | async-start | bytes 16777216 | tf_op jit(solution)/shard_map/all_to_all | solution.py:35
  251.2 98.2 %all-to-all-start.3 = ((bf16[4,256,4096]{2,0,1:T(4,128)(2,1)}), bf16[4,256,4096]{2,0,1:T(4,128)(2,1)}, u32[]{:S(2)}, u32[]{:S(2)}) async-start(bf16[4,256,4096]{2,0,1:T(4,128)(2,1)} %copy.115), calls=%async_computation.3 | async-start | bytes 16777216 | tf_op jit(solution)/shard_map/all_to_all | solution.py:30
  349.4 188.8 %all-to-all-start.2 = ((bf16[4,128,8192]{1,0,2:T(4,128)(2,1)}), bf16[4,128,8192]{1,0,2:T(4,128)(2,1)}, u32[]{:S(2)}, u32[]{:S(2)}) async-start(bf16[4,128,8192]{1,0,2:T(4,128)(2,1)} %copy.111), calls=%async_computation.2 | async-start | bytes 16777216 | tf_op jit(solution)/shard_map/all_to_all | solution.py:34
  354.4 514.3 %all-gather.9.cloned.1.call-start = ((), (), s32[]{:S(2)}) async-start(), calls=%async_computation.11 | async-start | bytes 25165824 | tf_op jit(solution)/shard_map/all_gather | solution.py:32
  538.2 99.4 %all-to-all-start.4 = ((bf16[8,128,4096]{2,1,0:T(8,128)(2,1)}), bf16[8,128,4096]{2,1,0:T(8,128)(2,1)}, u32[]{:S(2)}, u32[]{:S(2)}) async-start(bf16[8,128,4096]{2,1,0:T(8,128)(2,1)} %bitcast.62), calls=%async_computation.4 | async-start | bytes 16777216 | tf_op jit(solution)/shard_map/all_to_all | solution.py:42
  545.3 577.8 %all-gather.5.cloned.1.call-start = ((), (), s32[]{:S(2)}) async-start(), calls=%async_computation.9 | async-start | bytes 25165824 | tf_op jit(solution)/shard_map/all_gather | solution.py:51
  564.5 572.5 %all-gather.7.cloned.1.call-start = ((), (), s32[]{:S(2)}) async-start(), calls=%async_computation.10 | async-start | bytes 25165824 | tf_op jit(solution)/shard_map/all_gather | solution.py:52
  866.2 0.7 copy-start.1
  866.2 2.3 copy-start
  868.7 195.5 %all-to-all-start.6 = ((bf16[8,1024,1024]{2,1,0:T(8,128)(2,1)}), bf16[8,1024,1024]{2,1,0:T(8,128)(2,1)}, u32[]{:S(2)}, u32[]{:S(2)}) async-start(bf16[8,1024,1024]{2,1,0:T(8,128)(2,1)} %all-gather.9.cloned.1.call-done), calls=%async_computation.6 | async-start | bytes 33554432 | tf_op jit(solution)/shard_map/all_to_all | solution.py:49
  882.0 268.9 %all-gather.11.cloned.1.call-start = ((), (), s32[]{:S(2)}) async-start(), calls=%async_computation.12 | async-start | bytes 4718592 | tf_op jit(solution)/shard_map/all_gather | solution.py:76
  884.3 347.7 %reduce-scatter.2.cloned.1.call-start = ((), (), s32[]{:S(2)}) async-start(), calls=%async_computation.13 | async-start | bytes 4718592 | tf_op jit(solution)/shard_map/reduce_scatter | solution.py:80
  1164.4 20.1 %copy-start.2 = (f32[128,2]{0,1:T(2,128)S(1)}, f32[128,2]{0,1:T(2,128)}, u32[]{:S(2)}) copy-start(f32[128,2]{0,1:T(2,128)} %param.9) | copy-start | bytes 3076
Sparse Core Ops, SparseCore 0:
  363.8 198.2 all-gather.8
  564.7 198.4 all-gather.4
  866.3 195.8 all-gather.6
  1063.7 46.8 all-gather.10
  1184.3 47.5 reduce-scatter.1
where the time goes:
time: 1280 us; the launch traced here: 1270 us
  waiting for transfers between devices  599 us (47%)
  blocking collectives  300 us (23%)
  local copies, waits for them, and re-layouts  249 us (19%)
  starting transfers between devices  39.5 us (3%)
  matrix products  33.2 us (3%)
  other arithmetic  32.6 us (3%)
  between operations  14.4 us (1%)
    all_to_all x1, blocking collectives, body(): lax.all_to_all(lax.all_to_all(up_rows, 'tp', split_axis=0, concat_axis=2,...  187 us
    all_to_all x1, waiting for transfers between devices, body(): lax.all_to_all(down_whole, 'tp', split_axis=0, concat_axis=2, tiled=True)  180 us
    all_to_all x1, waiting for transfers between devices, body(): lax.all_to_all(lax.all_to_all(gate_rows, 'tp', split_axis=0, concat_axis=...  152 us
    all_to_all x1, blocking collectives, body(): lax.all_to_all(gate_local, 'gr', split_axis=1, concat_axis=0, tiled=True)  98.2 us
    all_to_all x1, waiting for transfers between devices, body(): lax.all_to_all(gate_rows, 'tp', split_axis=0, concat_axis=2, tiled=True)  79.9 us
    all_to_all x1, waiting for transfers between devices, body(): lax.all_to_all(up_rows, 'tp', split_axis=0, concat_axis=2, tiled=True)  73 us
    all_to_all x1, waiting for transfers between devices, body(): lax.all_to_all(up_local, 'gr', split_axis=1, concat_axis=0, tiled=True)  67.1 us
    all_to_all x2, local copies, waits for them, and re-layouts, body(): lax.all_to_all(down_whole, 'tp', split_axis=0, concat_axis=2, tiled=True)  58.8 us
  transfers between devices with their start and end apart: 10, of which 6 were waited for; matrix products, arithmetic and copies ran while one was open for 15% of the time, Pallas kernels for 0%

commit v1 on v0

--- a/solution.py
+++ b/solution.py
@@ -1,6 +1,10 @@
+import functools
+
 import jax
 import jax.numpy as jnp
 from jax import lax
+from jax.experimental import pallas as pl
+from jax.experimental.pallas import tpu as pltpu
 from jax.sharding import PartitionSpec as P
 
 EXPERTS = 8
@@ -18,13 +22,182 @@
     return stacked.transpose(0, 2, 1, 3, 4).reshape(local_experts, row_total, width)
 
 
-def body(prompt, expert_ids, route_weights, gate_master, up_master, down_master, ffn_gain):
+MESH = pl.DeviceIdType.MESH
+SPLIT = 2
+
+
+def exchange(shard_count, g_ref, u_ref, d_ref, *refs):
+    yg, yu, yd, xg, xu, xd, rg, ru = refs[:8]
+    y_send, y_recv, x_send, x_recv, z_send, z_recv = refs[8:]
+    group, shard, part = lax.axis_index("gr"), lax.axis_index("fs"), lax.axis_index("tp")
+    home = part == group
+    away = part != group
+    experts, rows, _ = g_ref.shape
+    width = rg.shape[2]
+    blocks = g_ref.shape[2] // width
+    step = experts // SPLIT
+    y_dev = (1 - group, shard, part)
+    x_dev = (group, shard, 1 - part)
+
+    barrier = pltpu.get_barrier_semaphore()
+    pl.semaphore_signal(barrier, inc=1, device_id=y_dev, device_id_type=MESH)
+    pl.semaphore_signal(barrier, inc=1, device_id=x_dev, device_id_type=MESH)
+    for hop in range(1, shard_count):
+        peer = lax.rem(shard + hop, shard_count)
+        pl.semaphore_signal(barrier, inc=1, device_id=(group, peer, part), device_id_type=MESH)
+    pl.semaphore_wait(barrier, shard_count + 1)
+
+    own, ys, xs, rs = (g_ref, u_ref, d_ref), (yg, yu, yd), (xg, xu, xd), (rg, ru)
+    pieces = [(a, k, j) for j in range(blocks) for k in range(SPLIT) for a in range(2)]
+    downs = [(2, k, j) for j in range(blocks) for k in range(SPLIT)]
+    d_rows = d_ref.shape[1] // blocks
+
+    def view(ref, a, k, j):
+        if a == 2:
+            return ref.at[pl.ds(k * step, step), pl.ds(j * d_rows, d_rows), :]
+        return ref.at[pl.ds(k * step, step), :, pl.ds(j * width, width)]
+
+    def y_copy(a, k, j):
+        return pltpu.make_async_remote_copy(
+            src_ref=view(own[a], a, k, j), dst_ref=view(ys[a], a, k, j),
+            send_sem=y_send.at[a, k, j], recv_sem=y_recv.at[a, k, j],
+            device_id=y_dev, device_id_type=MESH,
+        )
+
+    def x_copy(source, a, k, j):
+        return pltpu.make_async_remote_copy(
+            src_ref=view(source[a], a, k, j), dst_ref=view(xs[a], a, k, j),
+            send_sem=x_send.at[a, k, j], recv_sem=x_recv.at[a, k, j],
+            device_id=x_dev, device_id_type=MESH,
+        )
+
+    def z_copy(source, side, a, k, j):
+        columns_of = part if side == 0 else 1 - part
+        target = columns_of * blocks + j
+        copy = pltpu.make_async_remote_copy(
+            src_ref=view(source[a], a, k, j),
+            dst_ref=rs[a].at[pl.ds(k * step, step), pl.ds(pl.multiple_of(shard * rows, rows), rows), :],
+            send_sem=z_send.at[side, a, k, j], recv_sem=z_recv.at[a, k, shard],
+            device_id=(group, target, part), device_id_type=MESH,
+        )
+        return copy, target != shard
+
+    def deal(source, side, piece):
+        copy, leaves = z_copy(source, side, *piece)
+
+        @pl.when(leaves)
+        def _():
+            copy.start()
+
+    for piece in pieces + downs:
+        y_copy(*piece).start()
+
+    @pl.when(away)
+    def _():
+        for piece in pieces + downs:
+            x_copy(own, *piece).start()
+
+    @pl.when(home)
+    def _():
+        for piece in pieces:
+            deal(own, 0, piece)
+
+    for at, piece in enumerate(pieces):
+        y_copy(*piece).wait_recv()
+
+        @pl.when(home)
+        def _():
+            x_copy(ys, *piece).start()
+
+        @pl.when(away)
+        def _():
+            deal(ys, 0, piece)
+
+        if at:
+            x_copy(ys, *pieces[at - 1]).wait_recv()
+            deal(xs, 1, pieces[at - 1])
+    x_copy(ys, *pieces[-1]).wait_recv()
+    deal(xs, 1, pieces[-1])
+
+    for piece in downs:
+        y_copy(*piece).wait_recv()
+
+        @pl.when(home)
+        def _():
+            x_copy(ys, *piece).start()
+
+    for piece in downs:
+        x_copy(ys, *piece).wait_recv()
+    for piece in pieces + downs:
+        y_copy(*piece).wait_send()
+        x_copy(ys, *piece).wait_send()
+    for side in range(2):
+        for piece in pieces:
+            copy, leaves = z_copy(xs, side, *piece)
+
+            @pl.when(leaves)
+            def _():
+                copy.wait_send()
+
+    for a in range(2):
+        for k in range(SPLIT):
+            for peer in range(shard_count):
+                @pl.when(peer != shard)
+                def _():
+                    landed = rs[a].at[pl.ds(k * step, step), pl.ds(peer * rows, rows), :]
+                    pltpu.make_async_remote_copy(
+                        src_ref=landed, dst_ref=landed,
+                        send_sem=z_send.at[0, a, k, 0], recv_sem=z_recv.at[a, k, peer],
+                        device_id=x_dev, device_id_type=MESH,
+                    ).wait_recv()
+
+
+def handover(gate_local, up_local, down_local):
+    shard_count = lax.axis_size("fs")
+    part_count = lax.axis_size("tp")
+    group, shard, part = lax.axis_index("gr"), lax.axis_index("fs"), lax.axis_index("tp")
+    experts, rows, columns = gate_local.shape
+    blocks = shard_count // part_count
+    width = columns // blocks
+    like = [jax.ShapeDtypeStruct(a.shape, a.dtype) for a in (gate_local, up_local, down_local)]
+    dealt = jax.ShapeDtypeStruct((experts, rows * shard_count, width), gate_local.dtype)
+    yg, yu, yd, xg, xu, xd, rg, ru = pl.pallas_call(
+        functools.partial(exchange, shard_count),
+        out_shape=like + like + [dealt, dealt],
+        in_specs=[pl.BlockSpec(memory_space=pl.ANY)] * 3,
+        out_specs=[pl.BlockSpec(memory_space=pl.ANY)] * 8,
+        scratch_shapes=[
+            pltpu.SemaphoreType.DMA((3, SPLIT, blocks)),
+            pltpu.SemaphoreType.DMA((3, SPLIT, blocks)),
+            pltpu.SemaphoreType.DMA((3, SPLIT, blocks)),
+            pltpu.SemaphoreType.DMA((3, SPLIT, blocks)),
+            pltpu.SemaphoreType.DMA((2, 2, SPLIT, blocks)),
+            pltpu.SemaphoreType.DMA((2, SPLIT, shard_count)),
+        ],
+        compiler_params=pltpu.CompilerParams(collective_id=0, has_side_effects=True),
+    )(gate_local, up_local, down_local)
+    home = part == group
+    block = lax.rem(shard, blocks)
+    near = shard // blocks == part
+
+    def joined(own, over_y, over_x, landed):
+        cut = [lax.dynamic_slice_in_dim(a, block * width, width, 2) for a in (own, over_y, over_x)]
+        mine = jnp.where(near, jnp.where(home, cut[0], cut[1]), cut[2])
+        return lax.dynamic_update_slice_in_dim(landed, mine, shard * rows, 1)
+
+    gate_serving = joined(gate_local, yg, xg, rg)
+    up_serving = joined(up_local, yu, xu, ru)
+    near_down = jnp.where(home, down_local, yd)
+    first = part == 0
+    down_serving = jnp.concatenate(
+        [jnp.where(first, near_down, xd), jnp.where(first, xd, near_down)], axis=2
+    )
+    return gate_serving, up_serving, down_serving
+
+
+def general_handover(gate_local, up_local, down_local):
     group_count = lax.axis_size("gr")
     shard_count = lax.axis_size("fs")
-    folding = ffn_gain[None, :, None]
-    gate_local = (gate_master * folding).astype(jnp.bfloat16)
-    up_local = (up_master * folding).astype(jnp.bfloat16)
-    down_local = down_master.astype(jnp.bfloat16)
     gate_rows, up_rows = (
         lax.all_to_all(gate_local, "gr", split_axis=1, concat_axis=0, tiled=True),
         lax.all_to_all(up_local, "gr", split_axis=1, concat_axis=0, tiled=True),
@@ -53,6 +226,18 @@
     )
     gate_serving = regroup_rows(gate_joined, group_count, shard_count)
     up_serving = regroup_rows(up_joined, group_count, shard_count)
+    return gate_serving, up_serving, down_serving
+
+
+def body(prompt, expert_ids, route_weights, gate_master, up_master, down_master, ffn_gain):
+    folding = ffn_gain[None, :, None]
+    gate_local = (gate_master * folding).astype(jnp.bfloat16)
+    up_local = (up_master * folding).astype(jnp.bfloat16)
+    down_local = down_master.astype(jnp.bfloat16)
+    paired = lax.axis_size("gr") == 2 and lax.axis_size("tp") == 2
+    divides = lax.axis_size("fs") % 2 == 0 and gate_local.shape[0] % SPLIT == 0
+    move = handover if paired and divides else general_handover
+    gate_serving, up_serving, down_serving = move(gate_local, up_local, down_local)
     token_count = prompt.shape[0]
     local_experts = gate_serving.shape[0]
     xfloat = prompt.astype(jnp.float32)

time: 1280 us -> 1050 us (0.82)
  Pallas kernels: 0 us -> 571 us
  waiting for transfers between devices: 599 us -> 297 us
  blocking collectives: 300 us -> 16.1 us
  local copies, waits for them, and re-layouts: 249 us -> 45.5 us
  starting transfers between devices: 39.5 us -> 0.08 us
  other arithmetic: 32.6 us -> 65 us
    pallas_call x0 -> x1, Pallas kernels: none -> 571 us  [handover(): pl.pallas_call(functools.partial(exchange, shard_count), out_shape=like +...]
    all_to_all x5 -> x0, waiting for transfers between devices: 552 us -> none  [the longest x1 180 us: body(): lax.all_to_all(down_whole, 'tp', split_axis=0, concat_axis=2, tiled=True)]
    unnamed x5 -> x3, waiting for transfers between devices: 0.08 us -> 297 us
    all_to_all x2 -> x0, blocking collectives: 285 us -> none  [the longest x1 187 us: body(): lax.all_to_all(lax.all_to_all(up_rows, 'tp', split_axis=0, concat_axis=2,...]
    all_to_all x14 -> x0, local copies, waits for them, and re-layouts: 185 us -> none  [the longest x2 58.8 us: body(): lax.all_to_all(down_whole, 'tp', split_axis=0, concat_axis=2, tiled=True)]
    reduce_scatter x1 -> x0, waiting for transfers between devices: 47.2 us -> none  [body(): lax.psum_scatter(jnp.einsum('ecf,efd->ced', hidden, down_serving, preferr...]
    all_to_all x5 -> x0, starting transfers between devices: 39.2 us -> none  [the longest x1 13.3 us: body(): lax.all_to_all(down_whole, 'tp', split_axis=0, concat_axis=2, tiled=True)]
    unnamed x8 -> x15, local copies, waits for them, and re-layouts: 0.88 us -> 29.3 us
  transfers between devices with their start and end apart: 10 -> 2, of which waited for: 6 -> 1; matrix products, arithmetic and copies ran while one was open for 15% -> 5% of each run, Pallas kernels for 0% -> 55%
where the time goes in v1:
time: 1050 us
  Pallas kernels  571 us (54%)
  waiting for transfers between devices  297 us (28%)
  other arithmetic  65 us (6%)
  local copies, waits for them, and re-layouts  45.5 us (4%)
  matrix products  37.3 us (4%)
  blocking collectives  16.1 us (2%)
  between operations  14.9 us (1%)
    pallas_call x1, Pallas kernels, handover(): pl.pallas_call(functools.partial(exchange, shard_count), out_shape=like +...  571 us
    unnamed x3, waiting for transfers between devices  297 us
    unnamed x15, local copies, waits for them, and re-layouts  29.3 us
    dot_general x1, matrix products, body(): jnp.einsum('ecf,efd->ced', hidden, down_serving, preferred_element_type=j...  23.8 us
  transfers between devices with their start and end apart: 2, of which 1 were waited for; matrix products, arithmetic and copies ran while one was open for 5% of the time, Pallas kernels for 55%

profile of v1, /device:TPU:0, one launch (start us, length us, event | category | flops | bytes accessed | tf_op | source)
XLA Modules:
  0.0 1046.7 jit_solution(9966290256159608655)
XLA Ops:
  7.2 0.0 all-gather.2.cloned.1.call-start
  7.2 0.8 copy.30
  8.0 0.1 reshape.180
  8.1 0.1 eq.77
  8.3 0.6 reduce-window.6
  8.9 0.2 slice_reduce_fusion
  9.2 0.1 fusion.5
  9.3 0.2 and_reduce_fusion
  9.4 0.2 fusion.3
  9.6 0.1 reshape.184
  9.7 1.2 fusion.1
  10.9 1.2 fusion.2
  12.2 0.9 gather_fusion
  13.1 0.9 broadcast_select_fusion.3
  14.0 0.0 all-gather.2.cloned.1.call-update
  14.0 0.0 all-reduce.3.cloned.1.call-start
  14.1 0.0 copy-start.2
  14.1 9.1 convert_element_type.42.d_ref
  23.2 0.0 copy-done.2
  23.2 18.5 %multiply_convert_fusion = (bf16[4,256,4096]{2,1,0:T(8,128)(2,1)}, bf16[4,256,4096]{2,1,0:T(8,128)(2,1)}) fusion(f32[4,256,4096]{2,1,0:T(8,128)} %param.11, f32[256]{0:T(256)S(1)} %copy-done.2, f32[4,256,4096]{2,1,0:T(8,128)} %param.10), kind=kLoop, calls=%fused_computation.3 | loop fusion | flops 16777216 | bytes 50332672 | tf_op jit(solution)/shard_map/convert_element_type | solution.py:235
  41.7 571.2 %shard_map.102 = (bf16[4,256,4096]{2,1,0:T(8,128)(2,1)}, bf16[4,256,4096]{2,1,0:T(8,128)(2,1)}, bf16[4,1024,1024]{2,1,0:T(8,128)(2,1)}, bf16[4,256,4096]{2,1,0:T...) custom-call(bf16[4,256,4096]{2,1,0:T(8,128)(2,1)} %get-tuple-element, ...), custom_call_target="tpu_custom_call" | custom-call | tf_op jit(solution)/shard_map/pallas_call | solution.py:164
  612.9 0.0 copy-start
  612.9 10.1 select_dynamic-update-slice_fusion
  623.0 0.0 copy-done
  623.0 8.9 broadcast_select_fusion.2
  631.9 6.7 pad_maximum_fusion
  638.7 0.0 all-gather.2.cloned.1.call-done
  638.7 13.6 %fusion.15 = f32[4,256,1024]{2,1,0:T(8,128)} fusion(bf16[4,256,2048]{2,1,0:T(8,128)(2,1)} %all-gather.2.cloned.1.call-done, bf16[4,2048,1024]{2,1,0:T(8,128)(2,1)} %get-tuple-element.30), kind=kOutput, calls=%fused_computation.52 | convolution fusion | flops 4294967296 | bytes 25165824 | tf_op jit(solution)/shard_map/ecd,edf->ecf/dot_general | solution.py:262
  652.2 23.8 %convert_bitcast_fusion = bf16[256,4,2048]{0,2,1:T(8,128)(2,1)} fusion(bf16[4,1024,2048]{2,1,0:T(8,128)(2,1)} %pad_maximum_fusion, f32[4,256,1024]{2,1,0:T(8,128)} %fusion.15, bf16[4,256,2048]{2,1,0:T(8,128)(2,1)} %all-gather.2.cloned.1.call-done, bf16[4,2048,1024]{2,1,0:T(8,128)(2,1)} %get-tuple-element.31), kind=kOutput, calls=%fused_computation.8 | convolution fusion | flops 8598323200 | bytes 46137344 | tf_op jit(solution)/shard_map/ecf,efd->ced/dot_general | solution.py:266
  676.0 0.0 copy-start.4
  676.0 0.0 copy-start.1
  676.0 0.0 copy-start.3
  676.0 7.9 copy.33
  683.9 0.0 all-reduce.3.cloned.1.call-update
  683.9 0.0 copy-done.4
  683.9 0.6 dynamic-slice
  685.2 0.0 copy-done.1
  685.2 0.1 copy.34
  685.3 0.1 min.31
  685.4 0.1 copy.29
  685.6 0.0 copy-done.3
  685.6 0.1 copy.35
  685.7 296.6 %all-reduce.3.cloned.1.call-done = bf16[256,4,2048]{2,1,0:T(4,128)(2,1)} async-done(((bf16[256,4,2048]{2,1,0:T(4,128)(2,1)}), bf16[256,4,2048]{2,1,0:T(4,128)(2,1)}) %all-reduce.3.cloned.1.call-update) | async-done | bytes 4194320
  982.4 1.1 dynamic-slice_convert_fusion
  983.5 4.2 gather_fusion.1
  987.7 2.2 gather.10
  989.9 2.4 select_convert_fusion
  992.3 16.1 %all_to_all.4 = bf16[128,2,2048]{2,1,0:T(2,128)(2,1)S(1)} all-to-all(bf16[128,2,2048]{2,1,0:T(2,128)(2,1)S(1)} %select_convert_fusion), channel_id=1, replica_groups=mesh['gr'=2,'fs'=8,'tp'=2] {'tp'}, dimensions={0} | all-to-all | bytes 2097152 | tf_op jit(solution)/shard_map/all_to_all | solution.py:281
  1008.4 2.8 reduce_sum.52
  1011.2 0.8 reduce_sum.54
  1012.1 13.9 %copy.42 = bf16[4,2048,1024]{2,1,0:T(8,128)(2,1)} copy(bf16[4,2048,1024]{2,1,0:T(8,128)(2,1)} %get-tuple-element.30) | data formatting | bytes 33554432
  1026.0 13.9 %copy.43 = bf16[4,2048,1024]{2,1,0:T(8,128)(2,1)} copy(bf16[4,2048,1024]{2,1,0:T(8,128)(2,1)} %get-tuple-element.31) | data formatting | bytes 33554432
  (14 shorter events, 0.1 us)
Async XLA Ops:
  7.2 631.5 %all-gather.2.cloned.1.call-start = ((), (), s32[]{:S(2)}) async-start(), calls=%async_computation.1 | async-start | bytes 4718592 | tf_op jit(solution)/shard_map/all_gather | solution.py:261
  14.0 968.3 %all-reduce.3.cloned.1.call-start = ((), (), s32[]{:S(2)}) async-start(), calls=%async_computation.2 | async-start | bytes 8388608
  14.1 9.1 copy-start.2
  612.9 10.1 copy-start
  676.0 7.9 copy-start.4
  676.0 9.2 copy-start.1
  676.0 9.6 copy-start.3
Sparse Core Ops, SparseCore 0:
  14.1 416.0 all-gather.1
  684.0 298.2 all-reduce.2
